TPU v7x, 32 devices: a whole 2x2x4 slice. The times are simulated.
32 devices in a mesh: sp: 8 (over z, y), tp: 4 (over x, core).
Axes of the slice: x: 2, y: 2, z: 4, core: 2. Of those that a mesh axis runs over, the one named last changes fastest.
Arguments:
- normalized_sequence: bfloat16 [2048, 3072], P('sp', 'tp'), may hold values from -6 to 6
- probe_projection: bfloat16 [3072, 1024], P(None, 'tp'), may hold values from -0.109375 to 0.109375
- payload_array: bfloat16 [2048, 1024], P('sp', 'tp'), may hold values from -6 to 6
- onward_retain_scores: bfloat16 [2048, 1024], P('sp', 'tp'), may hold values from -5 to 5
- reverse_retain_scores: bfloat16 [2048, 1024], P('sp', 'tp'), may hold values from -5 to 5
- retention_slack: float32 [2, 1024], P(None, 'tp'), as said below
- additional_decay: float32 [2, 2048, 8], P(None, 'sp', 'tp'), may hold values from -1.38 to 0, as said below
- rescale_weights: float32 [1024], P('tp'), may hold values from 0.1 to 1.9
- result_cotangent: bfloat16 [2048, 1024], P('sp', 'tp'), may hold values from -6 to 6
Outputs:
- query_pre_grad: bfloat16 [2048, 1024], P('sp', 'tp')
- gate_fwd_grad: float32 [2048, 1024], P('sp', 'tp')
- gate_bwd_grad: float32 [2048, 1024], P('sp', 'tp')
- value_grad: bfloat16 [2048, 1024], P('sp', 'tp')
- query_weight_grad: float32 [3072, 1024], P('sp', 'tp')
Inputs may be any that keep to these rules, and one draw needn't show every extreme that they name: `retention_slack`: every entry is positive. `additional_decay`: zero except at a few positions.
All inputs are finite; a program needn't handle non-finite values.
Results may differ from a plain program's by a relative error of at most 0.025.
Values may be sent and summed in bfloat16 or wider, within the bound.
A program may use at most 64 MiB of HBM per device.

v0:
```python
import functools

import jax
import jax.numpy as jnp
from jax import lax
from jax.experimental import pallas as pl
from jax.experimental.pallas import tpu as pltpu
from jax.sharding import PartitionSpec as P

WIDTH = 128
EXTRA = 16
EPSILON = 1e-06
F32 = jnp.float32
BF16 = jnp.bfloat16


def dot(a, b, ca, cb):
    return lax.dot_general(a, b, (((ca,), (cb,)), ((), ())), preferred_element_type=F32)


def nn(a, b):
    return dot(a, b, 1, 0)


def nt(a, b):
    return dot(a, b, 1, 1)


def tn(a, b):
    return dot(a, b, 0, 0)


def split(a):
    hi = a.astype(BF16)
    return hi, (a - hi.astype(F32)).astype(BF16)


def split_dot(tri, a):
    hi, lo = split(a)
    return nn(tri, hi) + nn(tri, lo)


def sigmoid(x):
    return 1.0 / (1.0 + jnp.exp(-x))


def kernel(
    nsp,
    ntp,
    x_hbm,
    w_hbm,
    v_ref,
    f_ref,
    r_ref,
    slack_ref,
    decay_ref,
    gain_ref,
    cot_ref,
    dq_ref,
    gf_ref,
    gb_ref,
    dv_ref,
    wg_ref,
    xg,
    wv,
    msg1,
    got1,
    msg2,
    got2,
    acc,
    part,
    terms,
    run_s,
    dqs_s,
    loc_s,
    dk_s,
    local_sem,
    x_send,
    x_recv,
    a_send,
    a_recv,
    b_send,
    b_recv,
    c_send,
    c_recv,
):
    sp = lax.axis_index("sp")
    tp = lax.axis_index("tp")
    length, width = v_ref.shape
    heads = width // WIDTH
    feat = x_hbm.shape[1]
    rows = wg_ref.shape[0]
    half = length // 2

    own_x = pltpu.make_async_copy(x_hbm, xg.at[0], local_sem.at[0])
    own_w = pltpu.make_async_copy(w_hbm, wv, local_sem.at[1])
    own_x.start()
    own_w.start()

    barrier = pltpu.get_barrier_semaphore()

    @pl.loop(1, ntp)
    def _(o):
        pl.semaphore_signal(
            barrier, inc=1, device_id={"tp": lax.rem(tp + o, ntp)}, device_id_type=pl.DeviceIdType.MESH
        )

    @pl.loop(1, nsp)
    def _(o):
        pl.semaphore_signal(
            barrier, inc=1, device_id={"sp": lax.rem(sp + o, nsp)}, device_id_type=pl.DeviceIdType.MESH
        )

    pl.semaphore_wait(barrier, nsp + ntp - 2)

    def x_copy(o):
        return pltpu.make_async_remote_copy(
            src_ref=x_hbm,
            dst_ref=xg.at[o],
            send_sem=x_send.at[o],
            recv_sem=x_recv.at[o],
            device_id={"tp": lax.rem(tp + o, ntp)},
            device_id_type=pl.DeviceIdType.MESH,
        )

    @pl.loop(1, ntp)
    def _(o):
        x_copy(o).start()

    def state_copy(o, msg, got, send, recv, flipped):
        peer = lax.rem(sp + o, nsp)
        ahead = (sp + o) // nsp
        which = 1 - ahead if flipped else ahead
        return pltpu.make_async_remote_copy(
            src_ref=msg.at[which],
            dst_ref=got.at[o],
            send_sem=send.at[o],
            recv_sem=recv.at[o],
            device_id={"sp": peer},
            device_id_type=pl.DeviceIdType.MESH,
        )

    def first_copy(o):
        return state_copy(o, msg1, got1, a_send, a_recv, False)

    def second_copy(o):
        return state_copy(o, msg2, got2, b_send, b_recv, True)

    def term_copy(o):
        peer = lax.rem(sp + o, nsp)
        return pltpu.make_async_remote_copy(
            src_ref=part.at[pl.ds(pl.multiple_of(peer * rows, rows), rows)],
            dst_ref=terms.at[o],
            send_sem=c_send.at[o],
            recv_sem=c_recv.at[o],
            device_id={"sp": peer},
            device_id_type=pl.DeviceIdType.MESH,
        )

    row = lax.broadcasted_iota(jnp.int32, (length, length), 0)
    col = lax.broadcasted_iota(jnp.int32, (length, length), 1)
    masks = (row >= col, row <= col)
    tris = tuple(jnp.where(m, 1.0, 0.0).astype(BF16) for m in masks)
    strict = (
        jnp.where(row > col, 1.0, 0.0).astype(BF16),
        jnp.where(row < col, 1.0, 0.0).astype(BF16),
    )
    ends = (length - 1, 0)
    mids = (half - 1, half)
    gates = (f_ref, r_ref)

    def head(a, h):
        return a[:, h * WIDTH : (h + 1) * WIDTH]

    def keys_of(j):
        sig = sigmoid(-gates[j][...].astype(F32))
        return sig, slack_ref[j : j + 1, :] * sig

    values = v_ref[...]

    for j in range(2):
        _, keys = keys_of(j)
        spikes = jnp.concatenate(
            [jnp.broadcast_to(decay_ref[j, :, h : h + 1], (length, WIDTH)) for h in range(heads)], axis=1
        )
        running = split_dot(tris[j], jnp.log(1.0 - keys) + spikes)
        run_s[j] = running
        closing = running[ends[j] : ends[j] + 1]
        key_end = (keys * jnp.exp(closing - running)).astype(BF16)
        shrink = jnp.exp(closing)
        hi = shrink.astype(BF16).astype(F32)
        lo = shrink - hi
        place = lax.broadcasted_iota(jnp.int32, (EXTRA, WIDTH), 0)
        for h in range(heads):
            base = h * (WIDTH + EXTRA)
            msg1[j, base : base + WIDTH] = tn(head(values, h), head(key_end, h)).astype(BF16)
            tail = jnp.where(place == 0, head(hi, h), jnp.where(place == 1, head(lo, h), 0.0)).astype(BF16)
            msg1[j, base + WIDTH : base + WIDTH + EXTRA] = tail
            msg2[j, base + WIDTH : base + WIDTH + EXTRA] = tail

    @pl.loop(1, nsp)
    def _(o):
        first_copy(o).start()

    total = None
    own_w.wait()
    own_x.wait()
    for o in range(ntp):
        if o > 0:
            x_copy(o).wait_recv()
        owner = lax.rem(tp - o + ntp, ntp)
        term = nn(xg[o], wv[pl.ds(pl.multiple_of(owner * feat, feat), feat), :])
        total = term if total is None else total + term
    pre = total.astype(BF16).astype(F32)
    sig_q = sigmoid(pre)
    queries = pre * sig_q * WIDTH**-0.5
    slope = sig_q * (1.0 + pre * (1.0 - sig_q)) * WIDTH**-0.5

    def gather_states(copy_of, got, near, far):
        acc[...] = jnp.zeros_like(acc)
        ones = jnp.ones((heads, 1, WIDTH), F32)

        def one(o, weights):
            copy_of(o).wait_recv()
            new = []
            for h in range(heads):
                base = h * (WIDTH + EXTRA)
                tail = got[o, base + WIDTH : base + WIDTH + EXTRA].astype(F32)
                shrink = tail[0:1] + tail[1:2]
                lanes = slice(h * WIDTH, (h + 1) * WIDTH)
                state = got[o, base : base + WIDTH].astype(F32)

                @pl.when(o <= sp)
                def _():
                    acc[near, :, lanes] += weights[h] * state

                @pl.when(o > sp)
                def _():
                    acc[far, :, lanes] = shrink * acc[far, :, lanes] + state

                new.append(weights[h] * shrink)
            return tuple(new)

        lax.fori_loop(1, nsp, one, tuple(ones[h] for h in range(heads)))

    gather_states(first_copy, got1, 0, 1)
    entry = (acc[0], acc[1])
    entry_bf = tuple(e.astype(BF16) for e in entry)

    q_dec, k_dec, k_low, q_in = [], [], [], []
    for j in range(2):
        running = run_s[j]
        _, keys = keys_of(j)
        middle = running[mids[j] : mids[j] + 1]
        q_dec.append((queries * jnp.exp(running - middle)).astype(BF16))
        hi, lo = split(keys * jnp.exp(middle - running))
        k_dec.append(hi)
        k_low.append(lo)
        q_in.append((queries * jnp.exp(running)).astype(BF16))

    cot = cot_ref[...].astype(F32) * gain_ref[...]
    for h in range(heads):
        lanes = slice(h * WIDTH, (h + 1) * WIDTH)
        value = head(values, h)
        scores = None
        mixed = None
        for j in range(2):
            s = nt(head(q_dec[j], h), head(k_dec[j], h)) + nt(head(q_dec[j], h), head(k_low[j], h))
            s = jnp.where(masks[j], s, 0.0)
            scores = s if scores is None else scores + s
            m = nt(head(q_in[j], h), head(entry_bf[j], h))
            mixed = m if mixed is None else mixed + m
        scores, scores_low = split(scores)
        mixed = mixed + (nn(scores, value) + nn(scores_low, value))
        scale = lax.rsqrt(jnp.mean(mixed * mixed, axis=-1, keepdims=True) + EPSILON)
        normed = mixed * scale
        grad = cot[:, lanes]
        d_out = scale * (grad - normed * jnp.mean(grad * normed, axis=-1, keepdims=True))
        d_out, d_low = split(d_out)
        d_scores = nt(d_out, value) + nt(d_low, value)
        dq_total = jnp.zeros((length, WIDTH), F32)
        for j in range(2):
            base = h * (WIDTH + EXTRA)
            msg2[j, base : base + WIDTH] = tn(d_out, head(q_in[j], h)).astype(BF16)
            ds, ds_low = split(jnp.where(masks[j], d_scores, 0.0))
            dq_loc = nn(ds, head(k_dec[j], h))
            dk_loc = tn(ds, head(q_dec[j], h))
            dq_low = nn(ds_low, head(k_dec[j], h)) + nn(ds, head(k_low[j], h))
            dq_far = nn(d_out, head(entry_bf[j], h)) + nn(d_low, head(entry_bf[j], h))
            running = run_s[j, :, lanes]
            middle = running[mids[j] : mids[j] + 1]
            dq_total = dq_total + (dq_loc + dq_low) * jnp.exp(running - middle) + dq_far * jnp.exp(running)
            qd = head(q_dec[j], h).astype(F32)
            kd = head(k_dec[j], h).astype(F32)
            loc_s[j, :, lanes] = qd * dq_loc - kd * dk_loc + head(q_in[j], h).astype(F32) * dq_far
            dk_s[j, :, lanes] = dk_loc * jnp.exp(middle - running)
        dqs_s[:, lanes] = tn(scores, d_out)
        dq_ref[:, lanes] = (dq_total * slope[:, lanes]).astype(BF16)

    @pl.loop(1, nsp)
    def _(o):
        second_copy(o).start()

    dq = dq_ref[...]
    for o in range(ntp):
        owner = lax.rem(tp - o + ntp, ntp)
        part[pl.ds(pl.multiple_of(owner * feat, feat), feat), :] = tn(xg[o], dq).astype(BF16)

    @pl.loop(1, nsp)
    def _(o):
        term_copy(o).start()

    gather_states(second_copy, got2, 1, 0)
    dv = dqs_s[...]
    outs = (gf_ref, gb_ref)
    for j in range(2):
        leave = acc[j]
        leave_bf = leave.astype(BF16)
        running = run_s[j]
        closing = running[ends[j] : ends[j] + 1]
        sig, keys = keys_of(j)
        end_scale = jnp.exp(closing - running)
        key_end = keys * end_scale
        key_end_bf = key_end.astype(BF16)
        dk_far = jnp.concatenate([nn(head(values, h), head(leave_bf, h)) for h in range(heads)], axis=1)
        dv = dv + jnp.concatenate([nt(head(key_end_bf, h), head(leave_bf, h)) for h in range(heads)], axis=1)
        dk = dk_s[j] + end_scale * dk_far
        through = jnp.exp(closing) * jnp.sum(entry[j] * leave, axis=0, keepdims=True)
        d_log = split_dot(tris[1 - j], loc_s[j]) + split_dot(strict[j], key_end * dk_far) + through
        outs[j][...] = slack_ref[j : j + 1, :] * sig * (1.0 - sig) * (d_log / (1.0 - keys) - dk)
    dv_ref[...] = dv.astype(BF16)

    wg_ref[...] = part[pl.ds(pl.multiple_of(sp * rows, rows), rows), :].astype(F32)

    @pl.loop(1, nsp)
    def _(o):
        term_copy(o).wait_recv()
        wg_ref[...] += terms[o].astype(F32)

    @pl.loop(1, ntp)
    def _(o):
        x_copy(o).wait_send()

    @pl.loop(1, nsp)
    def _(o):
        first_copy(o).wait_send()
        second_copy(o).wait_send()
        term_copy(o).wait_send()


def on_device(nsp, ntp, x, w, v, f, r, slack, decay, gain, cot):
    length, width = v.shape
    heads = width // WIDTH
    feat = x.shape[1]
    depth = w.shape[0]
    rows = depth // nsp
    message = (heads * (WIDTH + EXTRA), WIDTH)
    vmem = pl.BlockSpec(memory_space=pltpu.VMEM)
    anywhere = pl.BlockSpec(memory_space=pl.ANY)
    shape = jax.ShapeDtypeStruct
    dma = pltpu.SemaphoreType.DMA
    return pl.pallas_call(
        functools.partial(kernel, nsp, ntp),
        out_shape=(
            shape((length, width), BF16),
            shape((length, width), F32),
            shape((length, width), F32),
            shape((length, width), BF16),
            shape((rows, width), F32),
        ),
        in_specs=[anywhere, anywhere] + [vmem] * 7,
        out_specs=(vmem,) * 5,
        scratch_shapes=[
            pltpu.VMEM((ntp, length, feat), BF16),
            pltpu.VMEM((depth, width), BF16),
            pltpu.VMEM((2,) + message, BF16),
            pltpu.VMEM((nsp,) + message, BF16),
            pltpu.VMEM((2,) + message, BF16),
            pltpu.VMEM((nsp,) + message, BF16),
            pltpu.VMEM((2, WIDTH, width), F32),
            pltpu.VMEM((depth, width), BF16),
            pltpu.VMEM((nsp, rows, width), BF16),
            pltpu.VMEM((2, length, width), F32),
            pltpu.VMEM((length, width), F32),
            pltpu.VMEM((2, length, width), F32),
            pltpu.VMEM((2, length, width), F32),
            dma((2,)),
            dma((ntp,)),
            dma((ntp,)),
            dma((nsp,)),
            dma((nsp,)),
            dma((nsp,)),
            dma((nsp,)),
            dma((nsp,)),
            dma((nsp,)),
        ],
        compiler_params=pltpu.CompilerParams(
            collective_id=0, has_side_effects=True, vmem_limit_bytes=50 * 1024 * 1024
        ),
    )(x, w, v, f, r, slack, decay, gain.reshape(1, width), cot)


def solution(mesh):
    placed = (
        P("sp", "tp"),
        P(None, "tp"),
        P("sp", "tp"),
        P("sp", "tp"),
        P("sp", "tp"),
        P(None, "tp"),
        P(None, "sp", "tp"),
        P("tp"),
        P("sp", "tp"),
    )
    return jax.shard_map(
        functools.partial(on_device, mesh.shape["sp"], mesh.shape["tp"]),
        mesh=mesh,
        in_specs=placed,
        out_specs=(P("sp", "tp"),) * 5,
        check_vma=False,
    )
```

profile of v0, /device:TPU:30, one launch (start us, length us, event | category | flops | bytes accessed | tf_op | source)
XLA Modules:
  0.0 82.7 jit_solution(7340175530836831177)
XLA Ops:
  0.6 0.8 copy.14.decay_ref
  1.5 0.0 copy-start
  1.5 1.4 %copy-done = bf16[3072,256]{1,0:T(8,128)(2,1)S(1)} copy-done((bf16[3072,256]{1,0:T(8,128)(2,1)S(1)}, bf16[3072,256]{1,0:T(8,128)(2,1)}, u32[]{:S(2)}) %copy-start) | copy-done | bytes 1572888
  2.9 0.0 copy-start.1
  2.9 1.0 %copy-done.1 = bf16[256,768]{1,0:T(8,128)(2,1)S(1)} copy-done((bf16[256,768]{1,0:T(8,128)(2,1)S(1)}, bf16[256,768]{1,0:T(8,128)(2,1)}, u32[]{:S(2)}) %copy-start.1) | copy-done | bytes 393240
  3.9 0.0 copy-start.2
  3.9 0.9 %copy-done.2 = bf16[256,256]{1,0:T(8,128)(2,1)S(1)} copy-done((bf16[256,256]{1,0:T(8,128)(2,1)S(1)}, bf16[256,256]{1,0:T(8,128)(2,1)}, u32[]{:S(2)}) %copy-start.2) | copy-done | bytes 131096
  4.8 0.0 copy-start.3
  4.8 0.9 %copy-done.3 = bf16[256,256]{1,0:T(8,128)(2,1)S(1)} copy-done((bf16[256,256]{1,0:T(8,128)(2,1)S(1)}, bf16[256,256]{1,0:T(8,128)(2,1)}, u32[]{:S(2)}) %copy-start.3) | copy-done | bytes 131096
  5.7 0.0 copy-start.4
  5.7 0.9 %copy-done.4 = bf16[256,256]{1,0:T(8,128)(2,1)S(1)} copy-done((bf16[256,256]{1,0:T(8,128)(2,1)S(1)}, bf16[256,256]{1,0:T(8,128)(2,1)}, u32[]{:S(2)}) %copy-start.4) | copy-done | bytes 131096
  6.6 0.0 copy-start.5
  6.6 0.9 %copy-done.5 = bf16[256,256]{1,0:T(8,128)(2,1)S(1)} copy-done((bf16[256,256]{1,0:T(8,128)(2,1)S(1)}, bf16[256,256]{1,0:T(8,128)(2,1)}, u32[]{:S(2)}) %copy-start.5) | copy-done | bytes 131096
  7.5 0.0 copy-start.6
  7.5 0.7 copy-done.6
  8.2 0.0 copy-start.7
  8.2 0.7 copy-done.7
  8.9 70.3 %shard_map.128 = (bf16[256,256]{1,0:T(8,128)(2,1)S(1)}, f32[256,256]{1,0:T(8,128)S(1)}, f32[256,256]{1,0:T(8,128)S(1)}, bf16[256,256]{1,0:T(8,128)(2,1)S(1)}, f32[384,256]{1,0:T(8,128)S(1)}) custom-call(bf16[256,768]{1,0:T(8,128)(2,1)S(1)} %copy-done.1, bf16[3072,256]{1,0:T(8,128)(2,1)S(1)} %copy-done, bf16[256,256]{1,0:T(8,128)(2,1)S(1)} %copy-done.2, ...), custom_call_target="tpu_custom_call" | custom-call | tf_op jit(solution)/shard_map/pallas_call | solution.py:362
  79.2 0.7 copy.20
  79.8 0.7 copy.21
  80.5 0.7 copy.22
  81.3 0.7 copy.23
  81.9 0.7 copy.24
Async XLA Ops:
  1.5 1.4 %copy-start = (bf16[3072,256]{1,0:T(8,128)(2,1)S(1)}, bf16[3072,256]{1,0:T(8,128)(2,1)}, u32[]{:S(2)}) copy-start(bf16[3072,256]{1,0:T(8,128)(2,1)} %w_hbm.1) | copy-start | bytes 4718596
  2.9 1.0 %copy-start.1 = (bf16[256,768]{1,0:T(8,128)(2,1)S(1)}, bf16[256,768]{1,0:T(8,128)(2,1)}, u32[]{:S(2)}) copy-start(bf16[256,768]{1,0:T(8,128)(2,1)} %x_hbm.1) | copy-start | bytes 1179652
  3.9 0.9 %copy-start.2 = (bf16[256,256]{1,0:T(8,128)(2,1)S(1)}, bf16[256,256]{1,0:T(8,128)(2,1)}, u32[]{:S(2)}) copy-start(bf16[256,256]{1,0:T(8,128)(2,1)} %v_ref.1) | copy-start | bytes 393220
  4.8 0.9 %copy-start.3 = (bf16[256,256]{1,0:T(8,128)(2,1)S(1)}, bf16[256,256]{1,0:T(8,128)(2,1)}, u32[]{:S(2)}) copy-start(bf16[256,256]{1,0:T(8,128)(2,1)} %f_ref.1) | copy-start | bytes 393220
  5.7 0.9 %copy-start.4 = (bf16[256,256]{1,0:T(8,128)(2,1)S(1)}, bf16[256,256]{1,0:T(8,128)(2,1)}, u32[]{:S(2)}) copy-start(bf16[256,256]{1,0:T(8,128)(2,1)} %r_ref.1) | copy-start | bytes 393220
  6.6 0.9 %copy-start.5 = (bf16[256,256]{1,0:T(8,128)(2,1)S(1)}, bf16[256,256]{1,0:T(8,128)(2,1)}, u32[]{:S(2)}) copy-start(bf16[256,256]{1,0:T(8,128)(2,1)} %cot_ref.1) | copy-start | bytes 393220
  7.5 0.7 copy-start.6
  8.2 0.7 copy-start.7
where the time goes:
time: 83.9 us; the launch traced here: 82.7 us
  Pallas kernels  70.3 us (84%)
  local copies, waits for them, and re-layouts  11.7 us (14%)
    pallas_call x1, Pallas kernels, on_device(): pl.pallas_call(functools.partial(kernel, nsp, ntp), out_shape=(shape((len...  70.3 us
    unnamed x22, local copies, waits for them, and re-layouts  11.7 us

commit v1 on v0

--- a/solution.py
+++ b/solution.py
@@ -49,6 +49,18 @@
     ntp,
     x_hbm,
     w_hbm,
+    v_hbm,
+    f_hbm,
+    r_hbm,
+    slack_hbm,
+    decay_hbm,
+    gain_hbm,
+    cot_hbm,
+    dq_ref,
+    gf_ref,
+    gb_ref,
+    dv_ref,
+    wg_ref,
     v_ref,
     f_ref,
     r_ref,
@@ -56,11 +68,6 @@
     decay_ref,
     gain_ref,
     cot_ref,
-    dq_ref,
-    gf_ref,
-    gb_ref,
-    dv_ref,
-    wg_ref,
     xg,
     wv,
     msg1,
@@ -86,14 +93,30 @@
 ):
     sp = lax.axis_index("sp")
     tp = lax.axis_index("tp")
-    length, width = v_ref.shape
+    length, width = v_hbm.shape
     heads = width // WIDTH
     feat = x_hbm.shape[1]
     rows = wg_ref.shape[0]
     half = length // 2
 
-    own_x = pltpu.make_async_copy(x_hbm, xg.at[0], local_sem.at[0])
+    own_x = pltpu.make_async_copy(x_hbm, xg.at[tp], local_sem.at[0])
     own_w = pltpu.make_async_copy(w_hbm, wv, local_sem.at[1])
+    small = [
+        pltpu.make_async_copy(source, target, local_sem.at[2 + i])
+        for i, (source, target) in enumerate(
+            (
+                (f_hbm, f_ref),
+                (r_hbm, r_ref),
+                (decay_hbm, decay_ref),
+                (slack_hbm, slack_ref),
+                (v_hbm, v_ref),
+                (gain_hbm, gain_ref),
+                (cot_hbm, cot_ref),
+            )
+        )
+    ]
+    for copy in small:
+        copy.start()
     own_x.start()
     own_w.start()
 
@@ -113,19 +136,25 @@
 
     pl.semaphore_wait(barrier, nsp + ntp - 2)
 
-    def x_copy(o):
+    chips = ntp // 2
+    chip, core = tp // 2, lax.rem(tp, 2)
+    sibling = chip * 2 + 1 - core
+
+    def x_copy(source, owner, place, target):
         return pltpu.make_async_remote_copy(
-            src_ref=x_hbm,
-            dst_ref=xg.at[o],
-            send_sem=x_send.at[o],
-            recv_sem=x_recv.at[o],
-            device_id={"tp": lax.rem(tp + o, ntp)},
+            src_ref=source,
+            dst_ref=xg.at[owner],
+            send_sem=x_send.at[place],
+            recv_sem=x_recv.at[owner],
+            device_id={"tp": target},
             device_id_type=pl.DeviceIdType.MESH,
         )
 
-    @pl.loop(1, ntp)
-    def _(o):
-        x_copy(o).start()
+    direct = [
+        x_copy(x_hbm, tp, i, lax.rem(chip + i, chips) * 2 + core) for i in range(1, chips)
+    ] + [x_copy(x_hbm, tp, 0, sibling)]
+    for copy in direct:
+        copy.start()
 
     def state_copy(o, msg, got, send, recv, flipped):
         peer = lax.rem(sp + o, nsp)
@@ -176,6 +205,8 @@
         sig = sigmoid(-gates[j][...].astype(F32))
         return sig, slack_ref[j : j + 1, :] * sig
 
+    for copy in small:
+        copy.wait()
     values = v_ref[...]
 
     for j in range(2):
@@ -202,15 +233,25 @@
     def _(o):
         first_copy(o).start()
 
-    total = None
+    def project(owner):
+        return nn(xg[owner], wv[pl.ds(pl.multiple_of(owner * feat, feat), feat), :])
+
     own_w.wait()
     own_x.wait()
-    for o in range(ntp):
-        if o > 0:
-            x_copy(o).wait_recv()
-        owner = lax.rem(tp - o + ntp, ntp)
-        term = nn(xg[o], wv[pl.ds(pl.multiple_of(owner * feat, feat), feat), :])
-        total = term if total is None else total + term
+    total = project(tp)
+    x_copy(x_hbm, sibling, 0, sibling).wait_recv()
+    total = total + project(sibling)
+    passed = []
+    for i in range(1, chips):
+        owner = lax.rem(chip - i + chips, chips) * 2 + core
+        x_copy(x_hbm, owner, 0, sibling).wait_recv()
+        onward = x_copy(xg.at[owner], owner, chips + i, sibling)
+        onward.start()
+        passed.append(onward)
+        total = total + project(owner)
+        other = lax.rem(chip - i + chips, chips) * 2 + 1 - core
+        x_copy(x_hbm, other, 0, sibling).wait_recv()
+        total = total + project(other)
     pre = total.astype(BF16).astype(F32)
     sig_q = sigmoid(pre)
     queries = pre * sig_q * WIDTH**-0.5
@@ -303,8 +344,7 @@
 
     dq = dq_ref[...]
     for o in range(ntp):
-        owner = lax.rem(tp - o + ntp, ntp)
-        part[pl.ds(pl.multiple_of(owner * feat, feat), feat), :] = tn(xg[o], dq).astype(BF16)
+        part[o * feat : (o + 1) * feat, :] = tn(xg[o], dq).astype(BF16)
 
     @pl.loop(1, nsp)
     def _(o):
@@ -337,9 +377,8 @@
         term_copy(o).wait_recv()
         wg_ref[...] += terms[o].astype(F32)
 
-    @pl.loop(1, ntp)
-    def _(o):
-        x_copy(o).wait_send()
+    for copy in direct + passed:
+        copy.wait_send()
 
     @pl.loop(1, nsp)
     def _(o):
@@ -356,7 +395,7 @@
     rows = depth // nsp
     message = (heads * (WIDTH + EXTRA), WIDTH)
     vmem = pl.BlockSpec(memory_space=pltpu.VMEM)
-    anywhere = pl.BlockSpec(memory_space=pl.ANY)
+    anywhere = pl.BlockSpec(memory_space=pltpu.HBM)
     shape = jax.ShapeDtypeStruct
     dma = pltpu.SemaphoreType.DMA
     return pl.pallas_call(
@@ -368,9 +407,16 @@
             shape((length, width), BF16),
             shape((rows, width), F32),
         ),
-        in_specs=[anywhere, anywhere] + [vmem] * 7,
+        in_specs=[anywhere] * 9,
         out_specs=(vmem,) * 5,
         scratch_shapes=[
+            pltpu.VMEM((length, width), BF16),
+            pltpu.VMEM((length, width), BF16),
+            pltpu.VMEM((length, width), BF16),
+            pltpu.VMEM((2, width), F32),
+            pltpu.VMEM((2, length, heads), F32),
+            pltpu.VMEM((1, width), F32),
+            pltpu.VMEM((length, width), BF16),
             pltpu.VMEM((ntp, length, feat), BF16),
             pltpu.VMEM((depth, width), BF16),
             pltpu.VMEM((2,) + message, BF16),
@@ -384,7 +430,7 @@
             pltpu.VMEM((length, width), F32),
             pltpu.VMEM((2, length, width), F32),
             pltpu.VMEM((2, length, width), F32),
-            dma((2,)),
+            dma((9,)),
             dma((ntp,)),
             dma((ntp,)),
             dma((nsp,)),

time: 83.9 us -> 83.5 us (level); the launches traced: 82.7 us -> 83.2 us
  no operation moved by 1% of the time
where the time goes in v1:
time: 83.5 us; the launch traced here: 83.2 us
  Pallas kernels  70.8 us (85%)
  local copies, waits for them, and re-layouts  11.7 us (14%)
    pallas_call x1, Pallas kernels, on_device(): pl.pallas_call(functools.partial(kernel, nsp, ntp), out_shape=(shape((len...  70.8 us
    unnamed x22, local copies, waits for them, and re-layouts  11.7 us

profile of v1, /device:TPU:30, one launch (start us, length us, event | category | flops | bytes accessed | tf_op | source)
XLA Modules:
  0.0 83.2 jit_solution(10706019926662373687)
XLA Ops:
  0.6 0.8 copy.14.decay_hbm
  1.5 0.0 copy-start
  1.5 1.4 %copy-done = bf16[3072,256]{1,0:T(8,128)(2,1)S(1)} copy-done((bf16[3072,256]{1,0:T(8,128)(2,1)S(1)}, bf16[3072,256]{1,0:T(8,128)(2,1)}, u32[]{:S(2)}) %copy-start) | copy-done | bytes 1572888
  2.9 0.0 copy-start.1
  2.9 1.0 %copy-done.1 = bf16[256,768]{1,0:T(8,128)(2,1)S(1)} copy-done((bf16[256,768]{1,0:T(8,128)(2,1)S(1)}, bf16[256,768]{1,0:T(8,128)(2,1)}, u32[]{:S(2)}) %copy-start.1) | copy-done | bytes 393240
  3.9 0.0 copy-start.2
  3.9 0.9 %copy-done.2 = bf16[256,256]{1,0:T(8,128)(2,1)S(1)} copy-done((bf16[256,256]{1,0:T(8,128)(2,1)S(1)}, bf16[256,256]{1,0:T(8,128)(2,1)}, u32[]{:S(2)}) %copy-start.2) | copy-done | bytes 131096
  4.8 0.0 copy-start.3
  4.8 0.9 %copy-done.3 = bf16[256,256]{1,0:T(8,128)(2,1)S(1)} copy-done((bf16[256,256]{1,0:T(8,128)(2,1)S(1)}, bf16[256,256]{1,0:T(8,128)(2,1)}, u32[]{:S(2)}) %copy-start.3) | copy-done | bytes 131096
  5.7 0.0 copy-start.4
  5.7 0.9 %copy-done.4 = bf16[256,256]{1,0:T(8,128)(2,1)S(1)} copy-done((bf16[256,256]{1,0:T(8,128)(2,1)S(1)}, bf16[256,256]{1,0:T(8,128)(2,1)}, u32[]{:S(2)}) %copy-start.4) | copy-done | bytes 131096
  6.6 0.0 copy-start.5
  6.6 0.9 %copy-done.5 = bf16[256,256]{1,0:T(8,128)(2,1)S(1)} copy-done((bf16[256,256]{1,0:T(8,128)(2,1)S(1)}, bf16[256,256]{1,0:T(8,128)(2,1)}, u32[]{:S(2)}) %copy-start.5) | copy-done | bytes 131096
  7.5 0.0 copy-start.6
  7.5 0.7 copy-done.6
  8.2 0.0 copy-start.7
  8.2 0.7 copy-done.7
  8.9 70.8 %shard_map.128 = (bf16[256,256]{1,0:T(8,128)(2,1)S(1)}, f32[256,256]{1,0:T(8,128)S(1)}, f32[256,256]{1,0:T(8,128)S(1)}, bf16[256,256]{1,0:T(8,128)(2,1)S(1)}, f32[384,256]{1,0:T(8,128)S(1)}) custom-call(bf16[256,768]{1,0:T(8,128)(2,1)S(1)} %copy-done.1, bf16[3072,256]{1,0:T(8,128)(2,1)S(1)} %copy-done, bf16[256,256]{1,0:T(8,128)(2,1)S(1)} %copy-done.2, ...), custom_call_target="tpu_custom_call" | custom-call | tf_op jit(solution)/shard_map/pallas_call | solution.py:401
  79.7 0.7 copy.20
  80.4 0.7 copy.21
  81.1 0.7 copy.22
  81.8 0.7 copy.23
  82.4 0.7 copy.24
Async XLA Ops:
  1.5 1.4 %copy-start = (bf16[3072,256]{1,0:T(8,128)(2,1)S(1)}, bf16[3072,256]{1,0:T(8,128)(2,1)}, u32[]{:S(2)}) copy-start(bf16[3072,256]{1,0:T(8,128)(2,1)} %w_hbm.1) | copy-start | bytes 4718596
  2.9 1.0 %copy-start.1 = (bf16[256,768]{1,0:T(8,128)(2,1)S(1)}, bf16[256,768]{1,0:T(8,128)(2,1)}, u32[]{:S(2)}) copy-start(bf16[256,768]{1,0:T(8,128)(2,1)} %x_hbm.1) | copy-start | bytes 1179652
  3.9 0.9 %copy-start.2 = (bf16[256,256]{1,0:T(8,128)(2,1)S(1)}, bf16[256,256]{1,0:T(8,128)(2,1)}, u32[]{:S(2)}) copy-start(bf16[256,256]{1,0:T(8,128)(2,1)} %v_hbm.1) | copy-start | bytes 393220
  4.8 0.9 %copy-start.3 = (bf16[256,256]{1,0:T(8,128)(2,1)S(1)}, bf16[256,256]{1,0:T(8,128)(2,1)}, u32[]{:S(2)}) copy-start(bf16[256,256]{1,0:T(8,128)(2,1)} %f_hbm.1) | copy-start | bytes 393220
  5.7 0.9 %copy-start.4 = (bf16[256,256]{1,0:T(8,128)(2,1)S(1)}, bf16[256,256]{1,0:T(8,128)(2,1)}, u32[]{:S(2)}) copy-start(bf16[256,256]{1,0:T(8,128)(2,1)} %r_hbm.1) | copy-start | bytes 393220
  6.6 0.9 %copy-start.5 = (bf16[256,256]{1,0:T(8,128)(2,1)S(1)}, bf16[256,256]{1,0:T(8,128)(2,1)}, u32[]{:S(2)}) copy-start(bf16[256,256]{1,0:T(8,128)(2,1)} %cot_hbm.1) | copy-start | bytes 393220
  7.5 0.7 copy-start.6
  8.2 0.7 copy-start.7

commit v2 on v1

--- a/solution.py
+++ b/solution.py
@@ -343,12 +343,18 @@
         second_copy(o).start()
 
     dq = dq_ref[...]
+    share = nsp // ntp
     for o in range(ntp):
-        part[o * feat : (o + 1) * feat, :] = tn(xg[o], dq).astype(BF16)
-
-    @pl.loop(1, nsp)
-    def _(o):
-        term_copy(o).start()
+        block = lax.rem(sp // share + 1 + o, ntp)
+        part[pl.ds(pl.multiple_of(block * feat, feat), feat), :] = tn(xg[block], dq).astype(BF16)
+
+        @pl.loop(0, share)
+        def _(i):
+            ahead = lax.rem(block * share + i - sp + nsp, nsp)
+
+            @pl.when(ahead > 0)
+            def _():
+                term_copy(ahead).start()
 
     gather_states(second_copy, got2, 1, 0)
     dv = dqs_s[...]

time: 83.5 us -> 83.5 us (level)
  no operation moved by 1% of the time
where the time goes in v2:
time: 83.5 us; the launch traced here: 83.2 us
  Pallas kernels  70.8 us (85%)
  local copies, waits for them, and re-layouts  11.7 us (14%)
    pallas_call x1, Pallas kernels, on_device(): pl.pallas_call(functools.partial(kernel, nsp, ntp), out_shape=(shape((len...  70.8 us
    unnamed x22, local copies, waits for them, and re-layouts  11.7 us

profile of v2, /device:TPU:30, one launch (start us, length us, event | category | flops | bytes accessed | tf_op | source)
XLA Modules:
  0.0 83.2 jit_solution(8108328527578851378)
XLA Ops:
  0.6 0.8 copy.14.decay_hbm
  1.5 0.0 copy-start
  1.5 1.4 %copy-done = bf16[3072,256]{1,0:T(8,128)(2,1)S(1)} copy-done((bf16[3072,256]{1,0:T(8,128)(2,1)S(1)}, bf16[3072,256]{1,0:T(8,128)(2,1)}, u32[]{:S(2)}) %copy-start) | copy-done | bytes 1572888
  2.9 0.0 copy-start.1
  2.9 1.0 %copy-done.1 = bf16[256,768]{1,0:T(8,128)(2,1)S(1)} copy-done((bf16[256,768]{1,0:T(8,128)(2,1)S(1)}, bf16[256,768]{1,0:T(8,128)(2,1)}, u32[]{:S(2)}) %copy-start.1) | copy-done | bytes 393240
  3.9 0.0 copy-start.2
  3.9 0.9 %copy-done.2 = bf16[256,256]{1,0:T(8,128)(2,1)S(1)} copy-done((bf16[256,256]{1,0:T(8,128)(2,1)S(1)}, bf16[256,256]{1,0:T(8,128)(2,1)}, u32[]{:S(2)}) %copy-start.2) | copy-done | bytes 131096
  4.8 0.0 copy-start.3
  4.8 0.9 %copy-done.3 = bf16[256,256]{1,0:T(8,128)(2,1)S(1)} copy-done((bf16[256,256]{1,0:T(8,128)(2,1)S(1)}, bf16[256,256]{1,0:T(8,128)(2,1)}, u32[]{:S(2)}) %copy-start.3) | copy-done | bytes 131096
  5.7 0.0 copy-start.4
  5.7 0.9 %copy-done.4 = bf16[256,256]{1,0:T(8,128)(2,1)S(1)} copy-done((bf16[256,256]{1,0:T(8,128)(2,1)S(1)}, bf16[256,256]{1,0:T(8,128)(2,1)}, u32[]{:S(2)}) %copy-start.4) | copy-done | bytes 131096
  6.6 0.0 copy-start.5
  6.6 0.9 %copy-done.5 = bf16[256,256]{1,0:T(8,128)(2,1)S(1)} copy-done((bf16[256,256]{1,0:T(8,128)(2,1)S(1)}, bf16[256,256]{1,0:T(8,128)(2,1)}, u32[]{:S(2)}) %copy-start.5) | copy-done | bytes 131096
  7.5 0.0 copy-start.6
  7.5 0.7 copy-done.6
  8.2 0.0 copy-start.7
  8.2 0.7 copy-done.7
  8.9 70.8 %shard_map.128 = (bf16[256,256]{1,0:T(8,128)(2,1)S(1)}, f32[256,256]{1,0:T(8,128)S(1)}, f32[256,256]{1,0:T(8,128)S(1)}, bf16[256,256]{1,0:T(8,128)(2,1)S(1)}, f32[384,256]{1,0:T(8,128)S(1)}) custom-call(bf16[256,768]{1,0:T(8,128)(2,1)S(1)} %copy-done.1, bf16[3072,256]{1,0:T(8,128)(2,1)S(1)} %copy-done, bf16[256,256]{1,0:T(8,128)(2,1)S(1)} %copy-done.2, ...), custom_call_target="tpu_custom_call" | custom-call | tf_op jit(solution)/shard_map/pallas_call | solution.py:407
  79.7 0.7 copy.20
  80.4 0.7 copy.21
  81.1 0.7 copy.22
  81.8 0.7 copy.23
  82.4 0.7 copy.24
Async XLA Ops:
  1.5 1.4 %copy-start = (bf16[3072,256]{1,0:T(8,128)(2,1)S(1)}, bf16[3072,256]{1,0:T(8,128)(2,1)}, u32[]{:S(2)}) copy-start(bf16[3072,256]{1,0:T(8,128)(2,1)} %w_hbm.1) | copy-start | bytes 4718596
  2.9 1.0 %copy-start.1 = (bf16[256,768]{1,0:T(8,128)(2,1)S(1)}, bf16[256,768]{1,0:T(8,128)(2,1)}, u32[]{:S(2)}) copy-start(bf16[256,768]{1,0:T(8,128)(2,1)} %x_hbm.1) | copy-start | bytes 1179652
  3.9 0.9 %copy-start.2 = (bf16[256,256]{1,0:T(8,128)(2,1)S(1)}, bf16[256,256]{1,0:T(8,128)(2,1)}, u32[]{:S(2)}) copy-start(bf16[256,256]{1,0:T(8,128)(2,1)} %v_hbm.1) | copy-start | bytes 393220
  4.8 0.9 %copy-start.3 = (bf16[256,256]{1,0:T(8,128)(2,1)S(1)}, bf16[256,256]{1,0:T(8,128)(2,1)}, u32[]{:S(2)}) copy-start(bf16[256,256]{1,0:T(8,128)(2,1)} %f_hbm.1) | copy-start | bytes 393220
  5.7 0.9 %copy-start.4 = (bf16[256,256]{1,0:T(8,128)(2,1)S(1)}, bf16[256,256]{1,0:T(8,128)(2,1)}, u32[]{:S(2)}) copy-start(bf16[256,256]{1,0:T(8,128)(2,1)} %r_hbm.1) | copy-start | bytes 393220
  6.6 0.9 %copy-start.5 = (bf16[256,256]{1,0:T(8,128)(2,1)S(1)}, bf16[256,256]{1,0:T(8,128)(2,1)}, u32[]{:S(2)}) copy-start(bf16[256,256]{1,0:T(8,128)(2,1)} %cot_hbm.1) | copy-start | bytes 393220
  7.5 0.7 copy-start.6
  8.2 0.7 copy-start.7
